TPU v7x, 256 devices: a whole 4x4x8 slice. The times are simulated.
256 devices in a mesh: sp: 32 (over z, x), fs: 4 (over y), tp: 2 (over core).
Axes of the slice: x: 4, y: 4, z: 8, core: 2. Of those that a mesh axis runs over, the one named last changes fastest.
Arguments:
- inputs: bfloat16 [4, 4096, 2048], P('fs', 'sp'), may hold values from -6 to 6
- input_norm_gain: bfloat16 [2048], replicated, may hold values from 0.099609375 to 1.8984375
- receptance_matrix: bfloat16 [2048, 1024], P('fs', 'tp'), may hold values from -0.125 to 0.125
- key_matrix: bfloat16 [2048, 1024], P('fs', 'tp'), may hold values from -0.125 to 0.125
- value_matrix: bfloat16 [2048, 1024], P('fs', 'tp'), may hold values from -0.125 to 0.125
- pooling_input_weight: bfloat16 [2048, 1024], P('fs', 'tp'), may hold values from -0.125 to 0.125
- decay_lower_matrix: bfloat16 [2048, 128], replicated, may hold values from -0.125 to 0.125
- decay_raise_matrix: bfloat16 [2, 64, 1024], P(None, None, 'tp'), may hold values from -1 to 1
- decay_offset_bias: float32 [2, 1024], P(None, 'tp'), may hold values from -13 to -3
- removal_lower_matrix: bfloat16 [2048, 128], replicated, may hold values from -0.125 to 0.125
- removal_raise_matrix: bfloat16 [2, 64, 1024], P(None, None, 'tp'), may hold values from -1 to 1
- removal_rate_bias: float32 [2, 1024], P(None, 'tp'), may hold values from -9 to 1.5
- tempo_scale: float32 [4, 2, 16, 4096], P('fs', None, 'tp', 'sp'), may hold values from 0.3 to 3.2, as said below
- sudden_decay_extra: float32 [4, 2, 16, 4096], P('fs', None, 'tp', 'sp'), may hold values from -2.8 to 0
- head_norm_gain: bfloat16 [1024], P('tp'), may hold values from 0.099609375 to 1.8984375
- group_mixing_weight: bfloat16 [4, 256, 256], P('tp'), may hold values from -0.375 to 0.375
- attention_output_matrix: bfloat16 [2048, 1024], P('fs', 'tp'), may hold values from -0.125 to 0.125
- pooling_output_matrix: bfloat16 [2048, 1024], P('fs', 'tp'), may hold values from -0.125 to 0.125
Outputs:
- mixed_out: bfloat16 [4, 4096, 2048], P('fs', ('sp', 'tp'))
Inputs may be any that keep to these rules, and one draw needn't show every extreme that they name: `tempo_scale`: positive.
All inputs are finite; a program needn't handle non-finite values.
Results may differ from a plain program's by a relative error of at most 0.017.
Values may be sent and summed in bfloat16 or wider, within the bound.
No kernel may reach another device: no remote copies, remote signals or barrier semaphores. Data moves between devices by JAX's collectives and lax.ppermute only.
A program may use at most 128 MiB of HBM per device.

v0:
```python
import jax
import jax.numpy as jnp
from jax import lax
from jax.sharding import Mesh
from jax.sharding import PartitionSpec as P

HEAD = 64
DECAY_RANK = 64
RATE_RANK = 64
POOL_GROUPS = 4
GROUP_WIDTH = 256
SP = ("sp_0", "sp_1")
SP_TP = ("sp_0", "sp_1", "tp")
norm_eps = 1e-06
head_eps = 0.00064
unit_eps = 1e-06
span_len = 32
highest = lax.Precision.HIGHEST


def filled_with(shard, identity):
    return jax.tree.map(
        lambda a, e: jnp.broadcast_to(jnp.asarray(e, a.dtype), a.shape), shard, identity
    )


def prefix_by_axis(shard, axes, combine, identity, reverse):
    before = start = filled_with(shard, identity)
    total = shard
    for axis in reversed(axes):
        peers, here = (lax.axis_size(axis), lax.axis_index(axis))
        pieces = jax.tree.map(
            lambda part, kind: lax.all_gather(part.astype(kind), axis),
            total,
            (jnp.bfloat16, jnp.bfloat16),
        )
        inside, total = (start, start)
        for k in reversed(range(peers)) if reverse else range(peers):
            passed = k > here if reverse else k < here
            total = combine(
                total, jax.tree.map(lambda part, own: part[k].astype(own.dtype), pieces, shard)
            )
            inside = jax.tree.map(lambda new, old: jnp.where(passed, new, old), total, inside)
        before = combine(inside, before)
    return before


def with_halo(cells, sides, width):
    for axis, dim in sides:
        count = lax.axis_size(axis)
        ends = count - 1
        head = lax.slice_in_dim(cells, 0, width, axis=dim)
        tail = lax.slice_in_dim(cells, cells.shape[dim] - width, cells.shape[dim], axis=dim)
        cells = jnp.concatenate(
            [
                lax.ppermute(tail, axis, [(i, (i + 1) % count) for i in range(ends)]),
                cells,
                lax.ppermute(head, axis, [((i + 1) % count, i) for i in range(ends)]),
            ],
            axis=dim,
        )
    return cells


def contract(form, left, right):
    return jnp.einsum(form, left, right, precision=highest)


def matmul(left, right):
    return contract("...ij,...jk->...ik", left, right)


def project(left, weight):
    return jnp.dot(left, weight, preferred_element_type=jnp.float32).astype(jnp.bfloat16)


def against(row_block, weight):
    return lax.dot_general(
        row_block, weight, (((1,), (1,)), ((), ())), preferred_element_type=jnp.float32
    )


def chain_combine(earlier, later):
    return (matmul(earlier[0], later[0]), matmul(earlier[1], later[0]) + later[1])


def unit_inverse(lower):
    result = jnp.eye(lower.shape[-1], dtype=jnp.float32) - lower
    power = lower
    for level in range(4):
        power = matmul(power, power)
        result = result + matmul(result, power)
    return result


def span_terms(logarithm_decay, unit, removal, written, value, recept):
    inner = jnp.cumsum(logarithm_decay, axis=-2)
    last = inner[..., -1:, :]
    ahead = unit * jnp.exp(inner - logarithm_decay)
    shrink = jnp.exp(-inner)
    remove_scaled = removal * shrink
    write_scaled = written * shrink
    query = recept * jnp.exp(inner)
    spots = jnp.arange(span_len)
    strict = spots[:, None] > spots[None, :]
    within = spots[:, None] >= spots[None, :]
    link_remove = jnp.where(strict, contract("...tk,...sk->...ts", ahead, remove_scaled), 0.0)
    link_write = jnp.where(strict, contract("...tk,...sk->...ts", ahead, write_scaled), 0.0)
    read_remove = jnp.where(within, contract("...tk,...sk->...ts", query, remove_scaled), 0.0)
    read_write = jnp.where(within, contract("...tk,...sk->...ts", query, write_scaled), 0.0)
    inverse = unit_inverse(link_remove)
    pull_map = -matmul(inverse, ahead)
    pull_base = -matmul(inverse, matmul(link_write, value))
    tail = jnp.exp(last - inner)
    remove_tail = removal * tail
    write_tail = written * tail
    transfer = jnp.eye(unit.shape[-1], dtype=jnp.float32) * jnp.exp(last) + contract(
        "...sk,...sj->...kj", pull_map, remove_tail
    )
    carried = contract("...sv,...sk->...vk", pull_base, remove_tail) + contract(
        "...sv,...sk->...vk", value, write_tail
    )
    query_eff = query + matmul(read_remove, pull_map)
    local_read = matmul(read_remove, pull_base) + matmul(read_write, value)
    return (query_eff, local_read, transfer, carried)


def shards(
    inputs,
    input_norm_gain,
    receptance_matrix,
    key_matrix,
    value_matrix,
    pooling_input_weight,
    decay_lower_matrix,
    decay_raise_matrix,
    decay_offset_bias,
    removal_lower_matrix,
    removal_raise_matrix,
    removal_rate_bias,
    tempo_scale,
    sudden_decay_extra,
    head_norm_gain,
    group_mixing_weight,
    attention_output_matrix,
    pooling_output_matrix,
):
    recept_full, key_full, value_full, pool_full, attn_full, pool_back = (
        lax.all_gather(receptance_matrix, "fs", axis=0, tiled=True),
        lax.all_gather(key_matrix, "fs", axis=0, tiled=True),
        lax.all_gather(value_matrix, "fs", axis=0, tiled=True),
        lax.all_gather(pooling_input_weight, "fs", axis=0, tiled=True),
        lax.all_gather(attention_output_matrix, "fs", axis=0, tiled=True),
        lax.all_gather(pooling_output_matrix, "fs", axis=0, tiled=True),
    )
    row_block = inputs[0].astype(jnp.float32)
    normed = (
        row_block
        * lax.rsqrt(jnp.mean(row_block * row_block, axis=-1, keepdims=True) + norm_eps)
        * input_norm_gain.astype(jnp.float32)
    ).astype(jnp.bfloat16)
    tokens = normed.shape[0]
    heads = recept_full.shape[1] // HEAD
    blocks = tokens // span_len
    receptance = project(normed, recept_full).astype(jnp.float32).reshape(tokens, heads, HEAD)
    key_rows = project(normed, key_full).astype(jnp.float32).reshape(tokens, heads, HEAD)
    val_rows = project(normed, value_full).astype(jnp.float32).reshape(tokens, heads, HEAD)
    pool_in = project(normed, pool_full)
    decay_act = jnp.tanh(project(normed, decay_lower_matrix).astype(jnp.float32)).astype(
        jnp.bfloat16
    )
    rate_latent = project(normed, removal_lower_matrix)
    unit_keys = key_rows * lax.rsqrt(
        jnp.sum(key_rows * key_rows, axis=-1, keepdims=True) + unit_eps
    )
    decays = []
    removals = []
    writes = []
    for travel_direction in range(2):
        part = decay_act[:, travel_direction * DECAY_RANK : (travel_direction + 1) * DECAY_RANK]
        decay_pre = decay_offset_bias[travel_direction] + jnp.dot(
            part, decay_raise_matrix[travel_direction], preferred_element_type=jnp.float32
        )
        decay_velocity = jnp.exp(-jax.nn.softplus(-decay_pre) - 0.5).reshape(tokens, heads, HEAD)
        decays.append(
            -decay_velocity * tempo_scale[0, travel_direction].T[:, :, None]
            + sudden_decay_extra[0, travel_direction].T[:, :, None]
        )
        latent = rate_latent[:, travel_direction * RATE_RANK : (travel_direction + 1) * RATE_RANK]
        rate = jax.nn.sigmoid(
            removal_rate_bias[travel_direction]
            + jnp.dot(
                latent, removal_raise_matrix[travel_direction], preferred_element_type=jnp.float32
            )
        )
        rate = rate.reshape(tokens, heads, HEAD)
        removals.append(unit_keys * rate)
        writes.append(key_rows * rate)

    def both_ways(forward, backward):
        stacked = jnp.stack([forward, jnp.flip(backward, axis=0)], axis=0)
        return stacked.reshape(2, blocks, span_len, heads, HEAD).transpose(0, 3, 1, 2, 4)

    query_eff, local_read, transfer, carried = span_terms(
        both_ways(decays[0], decays[1]),
        both_ways(unit_keys, unit_keys),
        both_ways(removals[0], removals[1]),
        both_ways(writes[0], writes[1]),
        both_ways(val_rows, val_rows),
        both_ways(receptance, receptance),
    )
    prefix_map, prefix_sum = lax.associative_scan(chain_combine, (transfer, carried), axis=2)
    total_map = prefix_map[:, :, -1]
    total_sum = prefix_sum[:, :, -1]
    identity_map = jnp.broadcast_to(jnp.eye(HEAD, dtype=jnp.float32), total_map.shape[1:])
    empty = jnp.zeros(total_map.shape[1:], jnp.float32)
    ahead_in = prefix_by_axis(
        (total_map[0], total_sum[0]), SP, chain_combine, (identity_map, empty), False
    )
    behind_in = prefix_by_axis(
        (total_map[1], total_sum[1]), SP, chain_combine, (identity_map, empty), True
    )
    incoming = jnp.stack([ahead_in[1], behind_in[1]], axis=0)
    ending = matmul(incoming[:, :, None], prefix_map) + prefix_sum
    starting = jnp.concatenate([incoming[:, :, None], ending[:, :, :-1]], axis=2)
    reads = contract("...tk,...vk->...tv", query_eff, starting) + local_read
    reads = reads.transpose(0, 2, 3, 1, 4).reshape(2, tokens, heads, HEAD)
    readout = reads[0] + jnp.flip(reads[1], axis=0)
    centred = readout - jnp.mean(readout, axis=-1, keepdims=True)
    spread = jnp.mean(centred * centred, axis=-1, keepdims=True)
    attn_out = (centred * lax.rsqrt(spread + head_eps)).reshape(
        tokens, heads * HEAD
    ) * head_norm_gain.astype(jnp.float32)
    attn_out = attn_out.astype(jnp.bfloat16)
    reach = 2 ** (POOL_GROUPS - 1)
    rimmed = with_halo(pool_in, ((SP, 0),), reach).astype(jnp.float32)
    position = lax.axis_index(SP) * tokens + jnp.arange(tokens)
    length = tokens * lax.axis_size(SP)
    running = rimmed
    window_sums = []
    window_counts = []
    for level in range(POOL_GROUPS):
        shift = 2**level
        running = running[:-shift] + running[shift:]
        window_sums.append(running[reach - shift : reach - shift + tokens])
        upper = jnp.minimum(position + shift, length)
        lower = jnp.maximum(position - shift, 0)
        window_counts.append((upper - lower).astype(jnp.float32))
    window_sums = jnp.stack(window_sums, axis=0)
    window_counts = jnp.stack(window_counts, axis=0)
    pool_vals = pool_in.astype(jnp.float32)
    groups_here = pool_in.shape[1] // GROUP_WIDTH
    diffs = []
    for member in range(groups_here):
        group = lax.axis_index("tp") * groups_here + member
        chosen = lax.dynamic_index_in_dim(
            window_sums[:, :, member * GROUP_WIDTH : (member + 1) * GROUP_WIDTH],
            group,
            0,
            keepdims=False,
        )
        count = lax.dynamic_index_in_dim(window_counts, group, 0, keepdims=False)
        diffs.append(
            chosen / count[:, None]
            - pool_vals[:, member * GROUP_WIDTH : (member + 1) * GROUP_WIDTH]
        )
    pool_diff = jnp.concatenate(diffs, axis=1).astype(jnp.bfloat16)
    mixed = [
        jnp.dot(
            pool_diff[:, member * GROUP_WIDTH : (member + 1) * GROUP_WIDTH],
            group_mixing_weight[member],
            preferred_element_type=jnp.float32,
        )
        for member in range(groups_here)
    ]
    pool_out = jnp.concatenate(mixed, axis=1).astype(jnp.bfloat16)
    attn_half, pool_half = (
        lax.all_to_all(attn_out, "tp", split_axis=0, concat_axis=1, tiled=True),
        lax.all_to_all(pool_out, "tp", split_axis=0, concat_axis=1, tiled=True),
    )
    attn_whole, pool_whole = (
        lax.all_gather(attn_full, "tp", axis=1, tiled=True),
        lax.all_gather(pool_back, "tp", axis=1, tiled=True),
    )
    result = against(attn_half, attn_whole) + against(pool_half, pool_whole)
    return result.astype(jnp.bfloat16)[None]


def solution(mesh):
    split = Mesh(
        mesh.devices.reshape(8, 4, mesh.shape["fs"], mesh.shape["tp"]), ("sp_0", "sp_1", "fs", "tp")
    )
    in_specs = (
        P("fs", SP, None),
        P(),
        P("fs", "tp"),
        P("fs", "tp"),
        P("fs", "tp"),
        P("fs", "tp"),
        P(),
        P(None, None, "tp"),
        P(None, "tp"),
        P(),
        P(None, None, "tp"),
        P(None, "tp"),
        P("fs", None, "tp", SP),
        P("fs", None, "tp", SP),
        P("tp"),
        P("tp", None, None),
        P("fs", "tp"),
        P("fs", "tp"),
    )
    out_specs = P("fs", SP_TP, None)
    return jax.shard_map(
        shards, mesh=split, in_specs=in_specs, out_specs=out_specs, check_vma=False
    )
```

profile of v0, /device:TPU:7, one launch (start us, length us, event | category | flops | bytes accessed | tf_op | source)
XLA Modules:
  0.0 448.1 jit_solution(15655499817770157762)
XLA Ops:
  18.1 27.2 %all-gather.19.cloned.1.call-done = bf16[2048,512]{1,0:T(8,128)(2,1)} async-done(((bf16[512,512]{1,0:T(8,128)(2,1)}), bf16[2048,512]{1,0:T(8,128)(2,1)}) %all-gather.19.cloned.1.call-update) | async-done | bytes 2097168 | tf_op jit(solution)/shard_map/all_gather | solution.py:150
  45.3 2.1 fusion.29
  47.6 32.9 %all-gather.21.cloned.1.call-done = bf16[2048,512]{1,0:T(8,128)(2,1)} async-done(((bf16[512,512]{1,0:T(8,128)(2,1)}), bf16[2048,512]{1,0:T(8,128)(2,1)}) %all-gather.21.cloned.1.call-update) | async-done | bytes 2097168 | tf_op jit(solution)/shard_map/all_gather | solution.py:151
  80.5 2.1 fusion.28
  90.6 3.0 fusion.55
  93.6 3.0 convolution_select_fusion.2
  96.6 1.2 fusion.215
  97.8 1.2 fusion.216
  99.0 1.3 convolution_add_fusion.5
  100.3 1.2 fusion.217
  101.5 1.4 convolution_add_fusion.4
  102.9 2.2 fusion.218
  105.1 2.2 convolution_add_fusion.3
  107.3 4.0 convolution_select_fusion.1
  113.4 1.1 copy.129
  114.5 3.2 convolution_add_fusion.2
  117.8 1.8 convolution_negate_fusion.1
  119.6 1.2 fusion.61
  120.8 1.2 convolution_negate_fusion
  122.0 4.2 fusion.46
  126.3 5.0 %multiply_add_fusion = f32[2,8,4,64,64]{4,3,2,1,0:T(8,128)S(1)} fusion(f32[2,8,4,32,64]{4,3,2,1,0:T(8,128)S(1)} %convolution_negate_fusion.1, f32[2,8,4,64]{3,2,1,0:T(4,128)S(1)} %copy-done.59, f32[64,64]{1,0:T(8,128)S(1)} %fusion.167, f32[2,8,4,32,64]{4,1,2,3,0:T(8,128)} %copy-done.15), kind=kOutput, calls=%fused_computation.8 | convolution fusion | flops 101187584 | bytes 2129920 | tf_op jit(solution)/shard_map/...sk,...sj->...kj/dot_general | solution.py:66
  131.3 1.2 fusion.41
  133.3 4.0 convolution_add_fusion.1
  137.3 1.2 convolution_add_fusion.7
  139.2 1.2 pad_add_fusion
  140.4 1.5 fusion.13
  142.6 1.5 convolution_bitcast_fusion.3
  145.7 11.3 %pad.33 = f32[2,8,4,64,64]{4,3,2,1,0:T(8,128)} pad(f32[2,8,2,64,64]{4,3,2,1,0:T(8,128)S(1)} %copy-done.30, f32[]{:T(128)} %constant.27.clone.1), padding=0_0_0x0_0_0x1_0_1x0_0_0x0_0_0 | pad | bytes 1572868 | tf_op jit(solution)/shard_map/pad | solution.py:212
  157.1 11.2 %pad.32 = f32[2,8,4,64,64]{4,3,2,1,0:T(8,128)} pad(f32[2,8,2,64,64]{4,3,2,1,0:T(8,128)S(1)} %pad_maximum_fusion.1, f32[]{:T(128)} %constant.27.clone.1), padding=0_0_0x0_0_0x0_1_1x0_0_0x0_0_0 | pad | bytes 1572868 | tf_op jit(solution)/shard_map/pad | solution.py:212
  168.3 11.2 %pad.28 = f32[2,8,4,64,64]{4,3,2,1,0:T(8,128)} pad(f32[2,8,2,64,64]{4,3,2,1,0:T(8,128)S(1)} %pad_maximum_fusion, f32[]{:T(128)} %constant.27.clone.1), padding=0_0_0x0_0_0x0_1_1x0_0_0x0_0_0 | pad | bytes 1572868 | tf_op jit(solution)/shard_map/pad | solution.py:212
  179.6 16.7 %pad.29 = f32[2,8,4,64,64]{4,3,2,1,0:T(8,128)} pad(f32[2,8,2,64,64]{4,3,2,1,0:T(8,128)} %pad_add_fusion.1, f32[]{:T(128)} %constant.27.clone.1), padding=0_0_0x0_0_0x1_0_1x0_0_0x0_0_0 | pad | bytes 1572868 | tf_op jit(solution)/shard_map/pad | solution.py:212
  196.3 2.2 add_convert_fusion
  198.5 10.7 %all-gather.6 = bf16[4,8,1,64,64]{4,3,2,1,0:T(8,128)(2,1)S(1)} all-gather(bf16[1,8,1,64,64]{4,3,2,1,0:T(8,128)(2,1)S(1)} %get-tuple-element.24), channel_id=8, replica_groups=mesh['sp_0'=8,'sp_1'=4,'fs'=4,'tp'=2] {'sp_1'}, dimensions={0}, use_global_device_ids=true | all-gather | bytes 327680 | tf_op jit(solution)/shard_map/all_gather | solution.py:33
  209.2 1.9 fusion.200
  211.1 11.9 %all-gather.4 = bf16[4,8,1,64,64]{4,3,2,1,0:T(8,128)(2,1)S(1)} all-gather(bf16[1,8,1,64,64]{4,3,2,1,0:T(8,128)(2,1)S(1)} %get-tuple-element.22), channel_id=6, replica_groups=mesh['sp_0'=8,'sp_1'=4,'fs'=4,'tp'=2] {'sp_1'}, dimensions={0}, use_global_device_ids=true | all-gather | bytes 327680 | tf_op jit(solution)/shard_map/all_gather | solution.py:33
  225.7 22.8 %all-gather.7 = bf16[64,64,64]{2,1,0:T(8,128)(2,1)S(1)} all-gather(bf16[8,64,64]{2,1,0:T(8,128)(2,1)S(1)} %get-tuple-element.46), channel_id=9, replica_groups=mesh['sp_0'=8,'sp_1'=4,'fs'=4,'tp'=2] {'sp_0'}, dimensions={0}, use_global_device_ids=true | all-gather | bytes 589824 | tf_op jit(solution)/shard_map/all_gather | solution.py:33
  249.3 22.2 %all-gather.5 = bf16[64,64,64]{2,1,0:T(8,128)(2,1)S(1)} all-gather(bf16[8,64,64]{2,1,0:T(8,128)(2,1)S(1)} %get-tuple-element.48), channel_id=7, replica_groups=mesh['sp_0'=8,'sp_1'=4,'fs'=4,'tp'=2] {'sp_0'}, dimensions={0}, use_global_device_ids=true | all-gather | bytes 589824 | tf_op jit(solution)/shard_map/all_gather | solution.py:33
  273.1 10.5 %all-gather.2 = bf16[4,8,1,64,64]{4,3,2,1,0:T(8,128)(2,1)S(1)} all-gather(bf16[1,8,1,64,64]{4,3,2,1,0:T(8,128)(2,1)S(1)} %get-tuple-element.23), channel_id=4, replica_groups=mesh['sp_0'=8,'sp_1'=4,'fs'=4,'tp'=2] {'sp_1'}, dimensions={0}, use_global_device_ids=true | all-gather | bytes 327680 | tf_op jit(solution)/shard_map/all_gather | solution.py:33
  283.6 10.3 %all-gather = bf16[4,8,1,64,64]{4,3,2,1,0:T(8,128)(2,1)S(1)} all-gather(bf16[1,8,1,64,64]{4,3,2,1,0:T(8,128)(2,1)S(1)} %get-tuple-element.21), channel_id=2, replica_groups=mesh['sp_0'=8,'sp_1'=4,'fs'=4,'tp'=2] {'sp_1'}, dimensions={0}, use_global_device_ids=true | all-gather | bytes 327680 | tf_op jit(solution)/shard_map/all_gather | solution.py:33
  295.9 20.4 %all-gather.3 = bf16[64,64,64]{2,1,0:T(8,128)(2,1)S(1)} all-gather(bf16[8,64,64]{2,1,0:T(8,128)(2,1)S(1)} %get-tuple-element.50), channel_id=5, replica_groups=mesh['sp_0'=8,'sp_1'=4,'fs'=4,'tp'=2] {'sp_0'}, dimensions={0}, use_global_device_ids=true | all-gather | bytes 589824 | tf_op jit(solution)/shard_map/all_gather | solution.py:33
  317.2 21.5 %all-gather.1 = bf16[64,64,64]{2,1,0:T(8,128)(2,1)S(1)} all-gather(bf16[8,64,64]{2,1,0:T(8,128)(2,1)S(1)} %get-tuple-element.52), channel_id=3, replica_groups=mesh['sp_0'=8,'sp_1'=4,'fs'=4,'tp'=2] {'sp_0'}, dimensions={0}, use_global_device_ids=true | all-gather | bytes 589824 | tf_op jit(solution)/shard_map/all_gather | solution.py:33
  345.2 3.0 fusion.30
  348.6 2.1 fusion.14
  350.7 1.8 copy.91
  352.5 1.9 stack.75
  354.4 1.8 rev.22
  356.2 2.0 copy.92
  358.2 1.3 copy.94
  359.5 1.2 copy.93
  360.8 1.3 fusion.17
  363.4 3.1 convolution_select_fusion.3
  366.5 1.2 fusion.221
  367.7 3.1 convolution_select_fusion
  370.8 1.2 convolution_add_fusion.6
  372.1 2.0 convolution_add_fusion.8
  374.1 2.0 convolution_bitcast_fusion
  376.6 3.4 fusion.9
  382.4 2.1 fusion.214
  384.5 1.9 collective-permute-start.1
  386.4 5.5 %collective-permute-start = (bf16[8,512]{1,0:T(8,128)(2,1)S(1)}, bf16[8,512]{1,0:T(8,128)(2,1)S(1)}, u32[]{:S(2)}, u32[]{:S(2)}) collective-permute-start(bf16[8,512]{1,0:T(8,128)(2,1)S(1)} %get-tuple-element.34), channel_id=1, source_target_pairs={{0,8},{8,16},{16,24},{24,32},{32,40},{40,48},{48,56},{56,64},{64,7... | collective-permute-start | bytes 24584 | tf_op jit(solution)/shard_map/ppermute | solution.py:56
  391.9 35.5 %all_to_all.32 = bf16[2,64,512]{2,1,0:T(8,128)(2,1)S(1)} all-to-all(bf16[2,64,512]{2,1,0:T(8,128)(2,1)S(1)} %multiply_convert_fusion), channel_id=1, replica_groups=mesh['sp_0'=8,'sp_1'=4,'fs'=4,'tp'=2] {'tp'}, dimensions={0} | all-to-all | bytes 262144 | tf_op jit(solution)/shard_map/all_to_all | solution.py:278
  429.2 3.9 all_to_all.33
  433.1 3.6 fusion.222
  436.7 4.3 fusion.1
  (306 shorter events, 45.8 us)
Async XLA Ops:
  6.5 5.0 %copy-start = (bf16[2048,128]{1,0:T(8,128)(2,1)S(1)}, bf16[2048,128]{1,0:T(8,128)(2,1)}, u32[]{:S(2)}) copy-start(bf16[2048,128]{1,0:T(8,128)(2,1)} %param.24) | copy-start | bytes 1572868
  6.5 4.7 %copy-start.68 = (f32[2,512]{1,0:T(2,128)S(1)}, f32[2,512]{1,0:T(2,128)}, u32[]{:S(2)}) copy-start(f32[2,512]{1,0:T(2,128)} %param.26) | copy-start | bytes 12292
  6.5 4.7 %copy-start.67 = (bf16[2048]{0:T(1024)(128)(2,1)S(1)}, bf16[2048]{0:T(1024)(128)(2,1)}, u32[]{:S(2)}) copy-start(bf16[2048]{0:T(1024)(128)(2,1)} %param.19) | copy-start | bytes 12292
  6.5 4.7 %copy-start.5 = (bf16[1,128,2048]{2,1,0:T(8,128)(2,1)S(1)}, bf16[1,128,2048]{2,1,0:T(8,128)(2,1)}, u32[]{:S(2)}) copy-start(bf16[1,128,2048]{2,1,0:T(8,128)(2,1)} %param.18) | copy-start | bytes 1572868
  6.5 38.7 %all-gather.19.cloned.1.call-start = ((), (), s32[]{:S(2)}) async-start(), calls=%async_computation.3 | async-start | bytes 2621440 | tf_op jit(solution)/shard_map/all_gather | solution.py:150
  7.3 73.2 %all-gather.21.cloned.1.call-start = ((), (), s32[]{:S(2)}) async-start(), calls=%async_computation.4 | async-start | bytes 2621440 | tf_op jit(solution)/shard_map/all_gather | solution.py:151
  8.0 3.9 copy-start.74
  8.0 337.1 %all-gather.17.cloned.1.call-start = ((), (), s32[]{:S(2)}) async-start(), calls=%async_computation.2 | async-start | bytes 2621440 | tf_op jit(solution)/shard_map/all_gather | solution.py:149
  8.8 339.4 %all-gather.23.cloned.1.call-start = ((), (), s32[]{:S(2)}) async-start(), calls=%async_computation.5 | async-start | bytes 2621440 | tf_op jit(solution)/shard_map/all_gather | solution.py:153
  9.3 372.0 %all-gather.29.cloned.1.call-start = ((), (), s32[]{:S(2)}) async-start(), calls=%async_computation.8 | async-start | bytes 2621440 | tf_op jit(solution)/shard_map/all_gather | solution.py:154
  9.9 2.6 copy-start.65
  9.9 2.6 copy-start.66
  10.0 372.0 %all-gather.27.cloned.1.call-start = ((), (), s32[]{:S(2)}) async-start(), calls=%async_computation.7 | async-start | bytes 2621440 | tf_op jit(solution)/shard_map/all_gather | solution.py:152
  10.5 422.6 %all-gather.25.cloned.1.call-start = ((), (), s32[]{:S(2)}) async-start(), calls=%async_computation.6 | async-start | bytes 6291456 | tf_op jit(solution)/shard_map/all_gather | solution.py:282
  11.5 69.0 %copy-start.62 = (f32[128]{0:T(128)}, f32[128]{0:T(128)S(1)}, u32[]{:S(2)}) copy-start(f32[128]{0:T(128)S(1)} %add_rsqrt_fusion.2) | copy-start | bytes 1540
  15.0 1.9 copy-start.72
  93.6 4.2 copy-start.9
  93.6 13.7 %copy-start.7 = (f32[2,8,4,32,64]{4,1,2,3,0:T(8,128)}, f32[2,8,4,32,64]{4,1,2,3,0:T(8,128)S(1)}, u32[]{:S(2)}) copy-start(f32[2,8,4,32,64]{4,1,2,3,0:T(8,128)S(1)} %get-tuple-element.12) | copy-start | bytes 1572868
  93.6 28.4 %copy-start.15 = (f32[2,8,4,32,64]{4,1,2,3,0:T(8,128)}, f32[2,8,4,32,64]{4,1,2,3,0:T(8,128)S(1)}, u32[]{:S(2)}) copy-start(f32[2,8,4,32,64]{4,1,2,3,0:T(8,128)S(1)} %get-tuple-element.16) | copy-start | bytes 1572868
  114.5 17.9 %copy-start.22 = (f32[1,4,32,8,64]{4,2,1,3,0:T(8,128)}, f32[1,4,32,8,64]{4,2,1,3,0:T(8,128)S(1)}, u32[]{:S(2)}) copy-start(f32[1,4,32,8,64]{4,2,1,3,0:T(8,128)S(1)} %copy.129) | copy-start | bytes 786436
  117.8 1.8 copy-start.20
  119.6 6.7 %copy-start.11 = (f32[2,8,4,32,64]{4,3,2,1,0:T(8,128)}, f32[2,8,4,32,64]{4,3,2,1,0:T(8,128)S(1)}, u32[]{:S(2)}) copy-start(f32[2,8,4,32,64]{4,3,2,1,0:T(8,128)S(1)} %convolution_negate_fusion.1) | copy-start | bytes 1572868
  122.0 4.3 copy-start.13
  122.0 4.3 copy-start.59
  131.3 11.3 %copy-start.2 = (f32[2,8,4,64,64]{4,3,2,1,0:T(8,128)}, f32[2,8,4,64,64]{4,3,2,1,0:T(8,128)S(1)}, u32[]{:S(2)}) copy-start(f32[2,8,4,64,64]{4,3,2,1,0:T(8,128)S(1)} %multiply_add_fusion) | copy-start | bytes 3145732
  131.3 2.0 copy-start.29
  137.3 4.6 %copy-start.16 = (f32[2,8,4,64,64]{4,3,2,1,0:T(8,128)}, f32[2,8,4,64,64]{4,3,2,1,0:T(8,128)S(1)}, u32[]{:S(2)}) copy-start(f32[2,8,4,64,64]{4,3,2,1,0:T(8,128)S(1)} %convolution_add_fusion.1) | copy-start | bytes 3145732
  145.6 11.3 %slice-start.1 = ((f32[2,8,4,64,64]{4,3,2,1,0:T(8,128)}), f32[2,8,1,64,64]{4,3,2,1,0:T(8,128)S(1)}, s32[]{:S(2)}) async-start(f32[2,8,4,64,64]{4,3,2,1,0:T(8,128)} %copy-done.16), calls=%async_computation.11 | async-start | bytes 1048576 | tf_op jit(solution)/shard_map/slice | solution.py:212
  145.7 11.3 %copy-start.53 = (f32[2,8,1,64,64]{4,3,2,1,0:T(8,128)S(1)}, f32[2,8,1,64,64]{4,3,2,1,0:T(8,128)}, u32[]{:S(2)}) copy-start(f32[2,8,1,64,64]{4,3,2,1,0:T(8,128)} %fusion.13) | copy-start | bytes 786436
  157.0 11.2 %slice-start = ((f32[2,8,4,64,64]{4,3,2,1,0:T(8,128)}), f32[2,8,1,64,64]{4,3,2,1,0:T(8,128)S(1)}, s32[]{:S(2)}) async-start(f32[2,8,4,64,64]{4,3,2,1,0:T(8,128)} %copy-done.2), calls=%async_computation.10 | async-start | bytes 1048576 | tf_op jit(solution)/shard_map/slice | solution.py:212
  157.0 11.2 %copy-start.54 = (f32[2,8,1,64,64]{4,3,2,1,0:T(8,128)S(1)}, f32[2,8,1,64,64]{4,3,2,1,0:T(8,128)}, u32[]{:S(2)}) copy-start(f32[2,8,1,64,64]{4,3,2,1,0:T(8,128)} %convolution_bitcast_fusion.3) | copy-start | bytes 786436
  179.6 16.7 %copy-start.3 = (f32[2,8,4,64,64]{4,3,2,1,0:T(8,128)S(1)}, f32[2,8,4,64,64]{4,3,2,1,0:T(8,128)}, u32[]{:S(2)}) copy-start(f32[2,8,4,64,64]{4,3,2,1,0:T(8,128)} %pad.33) | copy-start | bytes 3145732
  196.3 12.9 %copy-start.18 = (f32[2,8,4,64,64]{4,3,2,1,0:T(8,128)S(1)}, f32[2,8,4,64,64]{4,3,2,1,0:T(8,128)}, u32[]{:S(2)}) copy-start(f32[2,8,4,64,64]{4,3,2,1,0:T(8,128)} %pad.28) | copy-start | bytes 3145732
  196.3 12.9 %copy-start.19 = (f32[2,8,4,64,64]{4,3,2,1,0:T(8,128)S(1)}, f32[2,8,4,64,64]{4,3,2,1,0:T(8,128)}, u32[]{:S(2)}) copy-start(f32[2,8,4,64,64]{4,3,2,1,0:T(8,128)} %pad.29) | copy-start | bytes 3145732
  224.5 24.6 %copy-start.33 = (f32[8,64,64]{2,1,0:T(8,128)}, f32[8,64,64]{2,1,0:T(8,128)S(1)}, u32[]{:S(2)}) copy-start(f32[8,64,64]{2,1,0:T(8,128)S(1)} %convolution_add_fusion.19) | copy-start | bytes 393220
  224.8 24.6 %copy-start.34 = (f32[8,64,64]{2,1,0:T(8,128)}, f32[8,64,64]{2,1,0:T(8,128)S(1)}, u32[]{:S(2)}) copy-start(f32[8,64,64]{2,1,0:T(8,128)S(1)} %convolution_add_fusion.18) | copy-start | bytes 393220
  294.4 22.3 %copy-start.45 = (f32[8,64,64]{2,1,0:T(8,128)}, f32[8,64,64]{2,1,0:T(8,128)S(1)}, u32[]{:S(2)}) copy-start(f32[8,64,64]{2,1,0:T(8,128)S(1)} %convolution_add_fusion.33) | copy-start | bytes 393220
  316.4 24.8 %copy-start.26 = (bf16[64,64,64]{2,1,0:T(8,128)(2,1)}, bf16[64,64,64]{2,1,0:T(8,128)(2,1)S(1)}, u32[]{:S(2)}) copy-start(bf16[64,64,64]{2,1,0:T(8,128)(2,1)S(1)} %all-gather.3) | copy-start | bytes 1572868
  338.7 2.5 copy-start.27
  340.1 2.1 copy-start.35
  340.4 1.8 copy-start.37
  342.6 2.5 copy-start.63
  348.2 88.5 %all-gather.31.cloned.1.call-start = ((), (), s32[]{:S(2)}) async-start(), calls=%async_computation.9 | async-start | bytes 6291456 | tf_op jit(solution)/shard_map/all_gather | solution.py:283
  358.1 2.6 copy-start.36
  358.1 2.6 copy-start.38
  358.1 2.6 copy-start.40
  358.1 2.6 copy-start.42
  358.2 2.6 copy-start.44
  358.2 2.6 copy-start.49
  358.2 2.6 copy-start.56
  358.2 4.0 copy-start.57
  359.5 3.1 copy-start.32
  359.5 3.1 copy-start.46
  359.5 3.1 copy-start.55
  360.8 2.2 copy-start.50
  363.4 3.1 copy-start.14
  367.7 3.1 copy-start.21
  367.7 3.1 copy-start.23
  372.0 2.1 copy-start.17
  374.1 2.0 copy-start.4
  381.8 10.1 %copy-start.64 = (f32[512]{0:T(512)S(1)}, f32[512]{0:T(512)}, u32[]{:S(2)}) copy-start(f32[512]{0:T(512)} %convert_element_type.431) | copy-start | bytes 6148
  384.5 43.0 %collective-permute-start.1 = (bf16[8,512]{1,0:T(8,128)(2,1)S(1)}, bf16[8,512]{1,0:T(8,128)(2,1)S(1)}, u32[]{:S(2)}, u32[]{:S(2)}) collective-permute-start(bf16[8,512]{1,0:T(8,128)(2,1)S(1)} %get-tuple-element.35), channel_id=1, source_target_pairs={{8,0},{16,8},{24,16},{32,24},{40,32},{48,40},{56,48},{64,56},{72,6... | collective-permute-start | bytes 24584 | tf_op jit(solution)/shard_map/ppermute | solution.py:58
  386.4 41.1 %collective-permute-start = (bf16[8,512]{1,0:T(8,128)(2,1)S(1)}, bf16[8,512]{1,0:T(8,128)(2,1)S(1)}, u32[]{:S(2)}, u32[]{:S(2)}) collective-permute-start(bf16[8,512]{1,0:T(8,128)(2,1)S(1)} %get-tuple-element.34), channel_id=1, source_target_pairs={{0,8},{8,16},{16,24},{24,32},{32,40},{40,48},{48,56},{56,64},{64,7... | collective-permute-start | bytes 24584 | tf_op jit(solution)/shard_map/ppermute | solution.py:56
  436.7 4.4 copy-start.1
  (24 other events, 28.0 us)
Sparse Core Ops, SparseCore 0:
  9.2 36.0 all-gather.18
  47.1 33.3 all-gather.20
  82.3 33.3 all-gather.16
  117.4 33.3 all-gather.22
  152.5 33.3 all-gather.28
  187.5 33.3 all-gather.26
  348.3 47.0 all-gather.24
  397.2 31.7 all-gather.30
where the time goes:
time: 454 us; the launch traced here: 448 us
  blocking collectives  170 us (37%)
  matrix products  97.3 us (21%)
  local copies, waits for them, and re-layouts  78.8 us (17%)
  waiting for transfers between devices  63.8 us (14%)
  between operations  15.5 us (3%)
  other arithmetic  15 us (3%)
  starting transfers between devices  8.1 us (2%)
    all_gather x8, blocking collectives, prefix_by_axis(): lax.all_gather(part.astype(kind), axis)  130 us
    dot_general x67, matrix products, contract(): return jnp.einsum(form, left, right, precision=highest)  77.8 us
    pad x4, local copies, waits for them, and re-layouts, shards(): lax.associative_scan(chain_combine, (transfer, carried), axis=2)  50.4 us
    all_to_all x1, blocking collectives, shards(): lax.all_to_all(attn_out, 'tp', split_axis=0, concat_axis=1, tiled=True)  35.5 us
    all_gather x1, waiting for transfers between devices, shards(): lax.all_gather(value_matrix, 'fs', axis=0, tiled=True)  32.9 us
    all_gather x1, waiting for transfers between devices, shards(): lax.all_gather(key_matrix, 'fs', axis=0, tiled=True)  27.2 us
    dot_general x6, matrix products, project(): jnp.dot(left, weight, preferred_element_type=jnp.float32)  10 us
    rev x12, local copies, waits for them, and re-layouts, both_ways(): stacked = jnp.stack([forward, jnp.flip(backward, axis=0)], axis=0)  9.63 us
  transfers between devices with their start and end apart: 10, of which 2 were waited for; matrix products, arithmetic and copies ran while one was open for 40% of the time, Pallas kernels for 0%

commit v1 on v0

--- a/solution.py
+++ b/solution.py
@@ -275,7 +275,10 @@
     ]
     pool_out = jnp.concatenate(mixed, axis=1).astype(jnp.bfloat16)
     attn_half, pool_half = (
-        lax.all_to_all(attn_out, "tp", split_axis=0, concat_axis=1, tiled=True),
+        jnp.concatenate(
+            lax.all_to_all(jnp.stack(jnp.split(attn_out, lax.axis_size("tp"), axis=0)), "tp", 0, 0),
+            axis=1,
+        ),
         lax.all_to_all(pool_out, "tp", split_axis=0, concat_axis=1, tiled=True),
     )
     attn_whole, pool_whole = (

time: 454 us -> 463 us (1.020)
  transfers between devices with their start and end apart: 10 -> 10, of which waited for: 2 -> 3; matrix products, arithmetic and copies ran while one was open for 40% -> 40% of each run, Pallas kernels for 0% -> 0%
where the time goes in v1:
time: 463 us; the launch traced here: 456 us
  blocking collectives  171 us (37%)
  matrix products  98 us (21%)
  local copies, waits for them, and re-layouts  81.4 us (18%)
  waiting for transfers between devices  67.3 us (15%)
  between operations  15.4 us (3%)
  other arithmetic  15.1 us (3%)
  starting transfers between devices  8.1 us (2%)
    all_gather x8, blocking collectives, prefix_by_axis(): lax.all_gather(part.astype(kind), axis)  131 us
    dot_general x67, matrix products, contract(): return jnp.einsum(form, left, right, precision=highest)  77.9 us
    pad x4, local copies, waits for them, and re-layouts, shards(): lax.associative_scan(chain_combine, (transfer, carried), axis=2)  50.3 us
    all_to_all x1, blocking collectives, shards(): lax.all_to_all(jnp.stack(jnp.split(attn_out, lax.axis_size('tp'), axis=0)...  35.6 us
    all_gather x1, waiting for transfers between devices, shards(): lax.all_gather(value_matrix, 'fs', axis=0, tiled=True)  32.9 us
    all_gather x1, waiting for transfers between devices, shards(): lax.all_gather(key_matrix, 'fs', axis=0, tiled=True)  27.2 us
    dot_general x6, matrix products, project(): jnp.dot(left, weight, preferred_element_type=jnp.float32)  10 us
    rev x12, local copies, waits for them, and re-layouts, both_ways(): stacked = jnp.stack([forward, jnp.flip(backward, axis=0)], axis=0)  9.63 us
  transfers between devices with their start and end apart: 10, of which 3 were waited for; matrix products, arithmetic and copies ran while one was open for 40% of the time, Pallas kernels for 0%

profile of v1, /device:TPU:7, one launch (start us, length us, event | category | flops | bytes accessed | tf_op | source)
XLA Modules:
  0.0 456.0 jit_solution(6429801316079691683)
XLA Ops:
  18.0 27.2 %all-gather.19.cloned.1.call-done = bf16[2048,512]{1,0:T(8,128)(2,1)} async-done(((bf16[512,512]{1,0:T(8,128)(2,1)}), bf16[2048,512]{1,0:T(8,128)(2,1)}) %all-gather.19.cloned.1.call-update) | async-done | bytes 2097168 | tf_op jit(solution)/shard_map/all_gather | solution.py:150
  45.3 2.1 fusion.29
  47.6 32.9 %all-gather.21.cloned.1.call-done = bf16[2048,512]{1,0:T(8,128)(2,1)} async-done(((bf16[512,512]{1,0:T(8,128)(2,1)}), bf16[2048,512]{1,0:T(8,128)(2,1)}) %all-gather.21.cloned.1.call-update) | async-done | bytes 2097168 | tf_op jit(solution)/shard_map/all_gather | solution.py:151
  80.5 2.1 fusion.28
  90.6 3.0 fusion.55
  93.6 3.0 convolution_select_fusion.2
  96.6 1.2 fusion.216
  97.8 1.2 fusion.217
  99.0 1.3 convolution_add_fusion.5
  100.3 1.2 fusion.218
  101.5 1.4 convolution_add_fusion.4
  102.9 2.2 fusion.219
  105.0 2.2 convolution_add_fusion.3
  107.2 4.0 convolution_select_fusion.1
  113.4 1.1 copy.129
  114.5 3.2 convolution_add_fusion.2
  117.8 1.8 convolution_negate_fusion.1
  119.6 1.2 fusion.61
  120.8 1.2 convolution_negate_fusion
  122.0 4.2 fusion.46
  126.2 5.0 %multiply_add_fusion = f32[2,8,4,64,64]{4,3,2,1,0:T(8,128)S(1)} fusion(f32[2,8,4,32,64]{4,3,2,1,0:T(8,128)S(1)} %convolution_negate_fusion.1, f32[2,8,4,64]{3,2,1,0:T(4,128)S(1)} %copy-done.55, f32[64,64]{1,0:T(8,128)S(1)} %fusion.168, f32[2,8,4,32,64]{4,1,2,3,0:T(8,128)} %copy-done.15), kind=kOutput, calls=%fused_computation.8 | convolution fusion | flops 101187584 | bytes 2129920 | tf_op jit(solution)/shard_map/...sk,...sj->...kj/dot_general | solution.py:66
  131.2 1.2 fusion.41
  133.2 4.0 convolution_add_fusion.1
  137.2 1.2 convolution_add_fusion.7
  140.2 1.5 fusion.13
  142.4 1.5 convolution_bitcast_fusion.3
  145.5 11.2 %pad.33 = f32[2,8,4,64,64]{4,3,2,1,0:T(8,128)} pad(f32[2,8,2,64,64]{4,3,2,1,0:T(8,128)S(1)} %copy-done.32, f32[]{:T(128)} %constant.27.clone.1), padding=0_0_0x0_0_0x1_0_1x0_0_0x0_0_0 | pad | bytes 1572868 | tf_op jit(solution)/shard_map/pad | solution.py:212
  156.9 11.2 %pad.32 = f32[2,8,4,64,64]{4,3,2,1,0:T(8,128)} pad(f32[2,8,2,64,64]{4,3,2,1,0:T(8,128)S(1)} %pad_maximum_fusion.1, f32[]{:T(128)} %constant.27.clone.1), padding=0_0_0x0_0_0x0_1_1x0_0_0x0_0_0 | pad | bytes 1572868 | tf_op jit(solution)/shard_map/pad | solution.py:212
  168.2 11.2 %pad.28 = f32[2,8,4,64,64]{4,3,2,1,0:T(8,128)} pad(f32[2,8,2,64,64]{4,3,2,1,0:T(8,128)S(1)} %pad_maximum_fusion, f32[]{:T(128)} %constant.27.clone.1), padding=0_0_0x0_0_0x0_1_1x0_0_0x0_0_0 | pad | bytes 1572868 | tf_op jit(solution)/shard_map/pad | solution.py:212
  179.3 16.7 %pad.29 = f32[2,8,4,64,64]{4,3,2,1,0:T(8,128)} pad(f32[2,8,2,64,64]{4,3,2,1,0:T(8,128)} %pad_add_fusion.1, f32[]{:T(128)} %constant.27.clone.1), padding=0_0_0x0_0_0x1_0_1x0_0_0x0_0_0 | pad | bytes 1572868 | tf_op jit(solution)/shard_map/pad | solution.py:212
  196.1 2.2 add_convert_fusion
  198.3 10.7 %all-gather.6 = bf16[4,8,1,64,64]{4,3,2,1,0:T(8,128)(2,1)S(1)} all-gather(bf16[1,8,1,64,64]{4,3,2,1,0:T(8,128)(2,1)S(1)} %get-tuple-element.26), channel_id=8, replica_groups=mesh['sp_0'=8,'sp_1'=4,'fs'=4,'tp'=2] {'sp_1'}, dimensions={0}, use_global_device_ids=true | all-gather | bytes 327680 | tf_op jit(solution)/shard_map/all_gather | solution.py:33
  209.0 1.8 fusion.201
  210.8 11.9 %all-gather.4 = bf16[4,8,1,64,64]{4,3,2,1,0:T(8,128)(2,1)S(1)} all-gather(bf16[1,8,1,64,64]{4,3,2,1,0:T(8,128)(2,1)S(1)} %get-tuple-element.24), channel_id=6, replica_groups=mesh['sp_0'=8,'sp_1'=4,'fs'=4,'tp'=2] {'sp_1'}, dimensions={0}, use_global_device_ids=true | all-gather | bytes 327680 | tf_op jit(solution)/shard_map/all_gather | solution.py:33
  225.5 23.0 %all-gather.7 = bf16[64,64,64]{2,1,0:T(8,128)(2,1)S(1)} all-gather(bf16[8,64,64]{2,1,0:T(8,128)(2,1)S(1)} %get-tuple-element.50), channel_id=9, replica_groups=mesh['sp_0'=8,'sp_1'=4,'fs'=4,'tp'=2] {'sp_0'}, dimensions={0}, use_global_device_ids=true | all-gather | bytes 589824 | tf_op jit(solution)/shard_map/all_gather | solution.py:33
  249.2 22.1 %all-gather.5 = bf16[64,64,64]{2,1,0:T(8,128)(2,1)S(1)} all-gather(bf16[8,64,64]{2,1,0:T(8,128)(2,1)S(1)} %get-tuple-element.52), channel_id=7, replica_groups=mesh['sp_0'=8,'sp_1'=4,'fs'=4,'tp'=2] {'sp_0'}, dimensions={0}, use_global_device_ids=true | all-gather | bytes 589824 | tf_op jit(solution)/shard_map/all_gather | solution.py:33
  273.2 10.5 %all-gather.2 = bf16[4,8,1,64,64]{4,3,2,1,0:T(8,128)(2,1)S(1)} all-gather(bf16[1,8,1,64,64]{4,3,2,1,0:T(8,128)(2,1)S(1)} %get-tuple-element.25), channel_id=4, replica_groups=mesh['sp_0'=8,'sp_1'=4,'fs'=4,'tp'=2] {'sp_1'}, dimensions={0}, use_global_device_ids=true | all-gather | bytes 327680 | tf_op jit(solution)/shard_map/all_gather | solution.py:33
  283.7 10.2 %all-gather = bf16[4,8,1,64,64]{4,3,2,1,0:T(8,128)(2,1)S(1)} all-gather(bf16[1,8,1,64,64]{4,3,2,1,0:T(8,128)(2,1)S(1)} %get-tuple-element.23), channel_id=2, replica_groups=mesh['sp_0'=8,'sp_1'=4,'fs'=4,'tp'=2] {'sp_1'}, dimensions={0}, use_global_device_ids=true | all-gather | bytes 327680 | tf_op jit(solution)/shard_map/all_gather | solution.py:33
  301.1 3.0 fusion.30
  304.1 21.9 %all-gather.3 = bf16[64,64,64]{2,1,0:T(8,128)(2,1)} all-gather(bf16[8,64,64]{2,1,0:T(8,128)(2,1)S(1)} %copy-done.53), channel_id=5, replica_groups=mesh['sp_0'=8,'sp_1'=4,'fs'=4,'tp'=2] {'sp_0'}, dimensions={0}, use_global_device_ids=true | all-gather | bytes 589824 | tf_op jit(solution)/shard_map/all_gather | solution.py:33
  326.1 1.8 copy.91
  327.8 1.9 stack.84
  329.7 1.8 rev.22
  331.5 2.0 copy.92
  333.5 2.1 copy.94
  335.6 2.0 copy.93
  338.8 1.2 fusion.214
  339.9 21.2 %all-gather.1 = bf16[64,64,64]{2,1,0:T(8,128)(2,1)S(1)} all-gather(bf16[8,64,64]{2,1,0:T(8,128)(2,1)S(1)} %get-tuple-element.56), channel_id=3, replica_groups=mesh['sp_0'=8,'sp_1'=4,'fs'=4,'tp'=2] {'sp_0'}, dimensions={0}, use_global_device_ids=true | all-gather | bytes 589824 | tf_op jit(solution)/shard_map/all_gather | solution.py:33
  365.3 1.7 fusion.16
  368.0 3.1 convolution_select_fusion.3
  371.1 1.2 fusion.222
  372.3 3.1 convolution_select_fusion
  375.4 1.2 convolution_add_fusion.6
  376.7 1.9 convolution_add_fusion.8
  378.6 2.2 convolution_bitcast_fusion
  381.3 3.4 fusion.9
  385.7 2.1 fusion.215
  387.8 1.9 collective-permute-start.1
  389.8 5.5 %collective-permute-start = (bf16[8,512]{1,0:T(8,128)(2,1)S(1)}, bf16[8,512]{1,0:T(8,128)(2,1)S(1)}, u32[]{:S(2)}, u32[]{:S(2)}) collective-permute-start(bf16[8,512]{1,0:T(8,128)(2,1)S(1)} %get-tuple-element.36), channel_id=1, source_target_pairs={{0,8},{8,16},{16,24},{24,32},{32,40},{40,48},{48,56},{56,64},{64,7... | collective-permute-start | bytes 24584 | tf_op jit(solution)/shard_map/ppermute | solution.py:56
  395.9 35.6 %all_to_all.21 = bf16[2,64,512]{2,1,0:T(8,128)(2,1)S(1)} all-to-all(bf16[2,64,512]{2,1,0:T(8,128)(2,1)S(1)} %copy.149), channel_id=1, replica_groups=mesh['sp_0'=8,'sp_1'=4,'fs'=4,'tp'=2] {'tp'}, dimensions={0} | all-to-all | bytes 262144 | tf_op jit(solution)/shard_map/all_to_all | solution.py:279
  433.2 3.8 all_to_all.22
  437.1 4.2 fusion.223
  441.2 3.4 all-gather.31.cloned.1.call-done
  444.7 4.3 fusion.1
  (302 shorter events, 49.0 us)
Async XLA Ops:
  6.5 5.0 %copy-start = (bf16[2048,128]{1,0:T(8,128)(2,1)S(1)}, bf16[2048,128]{1,0:T(8,128)(2,1)}, u32[]{:S(2)}) copy-start(bf16[2048,128]{1,0:T(8,128)(2,1)} %param.24) | copy-start | bytes 1572868
  6.5 4.7 %copy-start.64 = (f32[2,512]{1,0:T(2,128)S(1)}, f32[2,512]{1,0:T(2,128)}, u32[]{:S(2)}) copy-start(f32[2,512]{1,0:T(2,128)} %param.26) | copy-start | bytes 12292
  6.5 4.7 %copy-start.63 = (bf16[2048]{0:T(1024)(128)(2,1)S(1)}, bf16[2048]{0:T(1024)(128)(2,1)}, u32[]{:S(2)}) copy-start(bf16[2048]{0:T(1024)(128)(2,1)} %param.19) | copy-start | bytes 12292
  6.5 4.7 %copy-start.5 = (bf16[1,128,2048]{2,1,0:T(8,128)(2,1)S(1)}, bf16[1,128,2048]{2,1,0:T(8,128)(2,1)}, u32[]{:S(2)}) copy-start(bf16[1,128,2048]{2,1,0:T(8,128)(2,1)} %param.18) | copy-start | bytes 1572868
  6.5 38.7 %all-gather.19.cloned.1.call-start = ((), (), s32[]{:S(2)}) async-start(), calls=%async_computation.3 | async-start | bytes 2621440 | tf_op jit(solution)/shard_map/all_gather | solution.py:150
  7.3 73.2 %all-gather.21.cloned.1.call-start = ((), (), s32[]{:S(2)}) async-start(), calls=%async_computation.4 | async-start | bytes 2621440 | tf_op jit(solution)/shard_map/all_gather | solution.py:151
  8.0 3.9 copy-start.70
  8.0 293.1 %all-gather.17.cloned.1.call-start = ((), (), s32[]{:S(2)}) async-start(), calls=%async_computation.2 | async-start | bytes 2621440 | tf_op jit(solution)/shard_map/all_gather | solution.py:149
  8.8 356.0 %all-gather.23.cloned.1.call-start = ((), (), s32[]{:S(2)}) async-start(), calls=%async_computation.5 | async-start | bytes 2621440 | tf_op jit(solution)/shard_map/all_gather | solution.py:153
  9.3 375.9 %all-gather.27.cloned.1.call-start = ((), (), s32[]{:S(2)}) async-start(), calls=%async_computation.7 | async-start | bytes 2621440 | tf_op jit(solution)/shard_map/all_gather | solution.py:152
  9.9 2.6 copy-start.61
  9.9 2.6 copy-start.62
  10.0 385.4 %all-gather.29.cloned.1.call-start = ((), (), s32[]{:S(2)}) async-start(), calls=%async_computation.8 | async-start | bytes 2621440 | tf_op jit(solution)/shard_map/all_gather | solution.py:154
  10.5 426.6 %all-gather.25.cloned.1.call-start = ((), (), s32[]{:S(2)}) async-start(), calls=%async_computation.6 | async-start | bytes 6291456 | tf_op jit(solution)/shard_map/all_gather | solution.py:285
  11.5 69.0 %copy-start.58 = (f32[128]{0:T(128)}, f32[128]{0:T(128)S(1)}, u32[]{:S(2)}) copy-start(f32[128]{0:T(128)S(1)} %add_rsqrt_fusion.2) | copy-start | bytes 1540
  12.3 1.5 copy-start.69
  15.0 1.9 copy-start.68
  93.6 4.2 copy-start.9
  93.6 13.6 %copy-start.7 = (f32[2,8,4,32,64]{4,1,2,3,0:T(8,128)}, f32[2,8,4,32,64]{4,1,2,3,0:T(8,128)S(1)}, u32[]{:S(2)}) copy-start(f32[2,8,4,32,64]{4,1,2,3,0:T(8,128)S(1)} %get-tuple-element.14) | copy-start | bytes 1572868
  93.6 28.3 %copy-start.15 = (f32[2,8,4,32,64]{4,1,2,3,0:T(8,128)}, f32[2,8,4,32,64]{4,1,2,3,0:T(8,128)S(1)}, u32[]{:S(2)}) copy-start(f32[2,8,4,32,64]{4,1,2,3,0:T(8,128)S(1)} %get-tuple-element.18) | copy-start | bytes 1572868
  114.5 17.9 %copy-start.24 = (f32[1,4,32,8,64]{4,2,1,3,0:T(8,128)}, f32[1,4,32,8,64]{4,2,1,3,0:T(8,128)S(1)}, u32[]{:S(2)}) copy-start(f32[1,4,32,8,64]{4,2,1,3,0:T(8,128)S(1)} %copy.129) | copy-start | bytes 786436
  117.8 1.8 copy-start.22
  117.8 1.8 copy-start.30
  119.6 6.6 %copy-start.11 = (f32[2,8,4,32,64]{4,3,2,1,0:T(8,128)}, f32[2,8,4,32,64]{4,3,2,1,0:T(8,128)S(1)}, u32[]{:S(2)}) copy-start(f32[2,8,4,32,64]{4,3,2,1,0:T(8,128)S(1)} %convolution_negate_fusion.1) | copy-start | bytes 1572868
  121.9 4.2 copy-start.13
  121.9 4.2 copy-start.55
  131.2 11.2 %copy-start.2 = (f32[2,8,4,64,64]{4,3,2,1,0:T(8,128)}, f32[2,8,4,64,64]{4,3,2,1,0:T(8,128)S(1)}, u32[]{:S(2)}) copy-start(f32[2,8,4,64,64]{4,3,2,1,0:T(8,128)S(1)} %multiply_add_fusion) | copy-start | bytes 3145732
  131.2 2.0 copy-start.31
  137.2 4.5 copy-start.16
  143.9 1.6 copy-start.32
  145.5 11.2 %slice-start.1 = ((f32[2,8,4,64,64]{4,3,2,1,0:T(8,128)}), f32[2,8,1,64,64]{4,3,2,1,0:T(8,128)S(1)}, s32[]{:S(2)}) async-start(f32[2,8,4,64,64]{4,3,2,1,0:T(8,128)} %copy-done.16), calls=%async_computation.11 | async-start | bytes 1048576 | tf_op jit(solution)/shard_map/slice | solution.py:212
  145.5 11.2 %copy-start.49 = (f32[2,8,1,64,64]{4,3,2,1,0:T(8,128)S(1)}, f32[2,8,1,64,64]{4,3,2,1,0:T(8,128)}, u32[]{:S(2)}) copy-start(f32[2,8,1,64,64]{4,3,2,1,0:T(8,128)} %fusion.13) | copy-start | bytes 786436
  156.9 11.2 %slice-start = ((f32[2,8,4,64,64]{4,3,2,1,0:T(8,128)}), f32[2,8,1,64,64]{4,3,2,1,0:T(8,128)S(1)}, s32[]{:S(2)}) async-start(f32[2,8,4,64,64]{4,3,2,1,0:T(8,128)} %copy-done.2), calls=%async_computation.10 | async-start | bytes 1048576 | tf_op jit(solution)/shard_map/slice | solution.py:212
  156.9 11.2 %copy-start.50 = (f32[2,8,1,64,64]{4,3,2,1,0:T(8,128)S(1)}, f32[2,8,1,64,64]{4,3,2,1,0:T(8,128)}, u32[]{:S(2)}) copy-start(f32[2,8,1,64,64]{4,3,2,1,0:T(8,128)} %convolution_bitcast_fusion.3) | copy-start | bytes 786436
  179.3 16.7 %copy-start.3 = (f32[2,8,4,64,64]{4,3,2,1,0:T(8,128)S(1)}, f32[2,8,4,64,64]{4,3,2,1,0:T(8,128)}, u32[]{:S(2)}) copy-start(f32[2,8,4,64,64]{4,3,2,1,0:T(8,128)} %pad.33) | copy-start | bytes 3145732
  196.1 12.9 %copy-start.20 = (f32[2,8,4,64,64]{4,3,2,1,0:T(8,128)S(1)}, f32[2,8,4,64,64]{4,3,2,1,0:T(8,128)}, u32[]{:S(2)}) copy-start(f32[2,8,4,64,64]{4,3,2,1,0:T(8,128)} %pad.28) | copy-start | bytes 3145732
  196.1 12.9 %copy-start.21 = (f32[2,8,4,64,64]{4,3,2,1,0:T(8,128)S(1)}, f32[2,8,4,64,64]{4,3,2,1,0:T(8,128)}, u32[]{:S(2)}) copy-start(f32[2,8,4,64,64]{4,3,2,1,0:T(8,128)} %pad.29) | copy-start | bytes 3145732
  224.2 24.8 %copy-start.34 = (f32[8,64,64]{2,1,0:T(8,128)}, f32[8,64,64]{2,1,0:T(8,128)S(1)}, u32[]{:S(2)}) copy-start(f32[8,64,64]{2,1,0:T(8,128)S(1)} %convolution_add_fusion.19) | copy-start | bytes 393220
  224.5 24.8 %copy-start.36 = (f32[8,64,64]{2,1,0:T(8,128)}, f32[8,64,64]{2,1,0:T(8,128)S(1)}, u32[]{:S(2)}) copy-start(f32[8,64,64]{2,1,0:T(8,128)S(1)} %convolution_add_fusion.18) | copy-start | bytes 393220
  293.9 5.4 %copy-start.26 = (bf16[4,8,1,64,64]{4,3,2,1,0:T(8,128)(2,1)}, bf16[4,8,1,64,64]{4,3,2,1,0:T(8,128)(2,1)S(1)}, u32[]{:S(2)}) copy-start(bf16[4,8,1,64,64]{4,3,2,1,0:T(8,128)(2,1)S(1)} %all-gather) | copy-start | bytes 786436
  294.1 5.2 %copy-start.43 = (f32[8,64,64]{2,1,0:T(8,128)}, f32[8,64,64]{2,1,0:T(8,128)S(1)}, u32[]{:S(2)}) copy-start(f32[8,64,64]{2,1,0:T(8,128)S(1)} %fusion.130) | copy-start | bytes 393220
  299.3 1.8 copy-start.59
  301.1 3.0 copy-start.53
  333.5 4.1 copy-start.35
  333.5 4.1 copy-start.37
  333.5 4.1 copy-start.40
  333.5 4.1 copy-start.51
  333.5 4.2 copy-start.52
  333.5 5.3 %copy-start.42 = (f32[8,64,64]{2,1,0:T(8,128)S(1)}, f32[8,64,64]{2,1,0:T(8,128)}, u32[]{:S(2)}) copy-start(f32[8,64,64]{2,1,0:T(8,128)} %fusion.155) | copy-start | bytes 393220
  335.6 25.5 %copy-start.29 = (bf16[64,64,64]{2,1,0:T(8,128)(2,1)S(1)}, bf16[64,64,64]{2,1,0:T(8,128)(2,1)}, u32[]{:S(2)}) copy-start(bf16[64,64,64]{2,1,0:T(8,128)(2,1)} %all-gather.3) | copy-start | bytes 1572868
  364.8 79.9 %all-gather.31.cloned.1.call-start = ((), (), s32[]{:S(2)}) async-start(), calls=%async_computation.9 | async-start | bytes 6291456 | tf_op jit(solution)/shard_map/all_gather | solution.py:286
  365.3 2.7 copy-start.10
  365.3 2.7 copy-start.17
  365.3 2.7 copy-start.18
  368.0 3.1 copy-start.14
  372.3 3.1 copy-start.23
  372.3 3.1 copy-start.25
  376.7 1.9 copy-start.19
  376.7 1.9 copy-start.41
  378.6 2.2 copy-start.4
  387.8 7.6 %copy-start.60 = (f32[512]{0:T(512)S(1)}, f32[512]{0:T(512)}, u32[]{:S(2)}) copy-start(f32[512]{0:T(512)} %convert_element_type.430) | copy-start | bytes 6148
  387.8 43.7 %collective-permute-start.1 = (bf16[8,512]{1,0:T(8,128)(2,1)S(1)}, bf16[8,512]{1,0:T(8,128)(2,1)S(1)}, u32[]{:S(2)}, u32[]{:S(2)}) collective-permute-start(bf16[8,512]{1,0:T(8,128)(2,1)S(1)} %get-tuple-element.37), channel_id=1, source_target_pairs={{8,0},{16,8},{24,16},{32,24},{40,32},{48,40},{56,48},{64,56},{72,6... | collective-permute-start | bytes 24584 | tf_op jit(solution)/shard_map/ppermute | solution.py:58
  389.8 41.8 %collective-permute-start = (bf16[8,512]{1,0:T(8,128)(2,1)S(1)}, bf16[8,512]{1,0:T(8,128)(2,1)S(1)}, u32[]{:S(2)}, u32[]{:S(2)}) collective-permute-start(bf16[8,512]{1,0:T(8,128)(2,1)S(1)} %get-tuple-element.36), channel_id=1, source_target_pairs={{0,8},{8,16},{16,24},{24,32},{32,40},{40,48},{48,56},{56,64},{64,7... | collective-permute-start | bytes 24584 | tf_op jit(solution)/shard_map/ppermute | solution.py:56
  444.7 4.3 copy-start.1
  (20 other events, 20.2 us)
Sparse Core Ops, SparseCore 0:
  9.2 36.0 all-gather.18
  47.1 33.3 all-gather.20
  82.3 33.3 all-gather.16
  117.4 33.3 all-gather.22
  152.5 33.3 all-gather.26
  187.5 33.3 all-gather.28
  364.9 48.4 all-gather.24
  415.2 29.3 all-gather.30
